TPU v7x, 256 devices: a 4x2x16 block of a 4x16x16 slice. The times are simulated.
256 devices in a mesh: grp: 2 (over y), sp: 32 (over z, core), tp: 4 (over x).
Axes of the slice: x: 4, y: 2, z: 16, core: 2. Of those that a mesh axis runs over, the one named last changes fastest.
The devices are a block of a 4x16x16 slice.
Arguments:
- queries: bfloat16 [8192, 512], P(('grp', 'sp'), 'tp'), parts along dimension 0, may hold values from -6 to 6
- key_rows: bfloat16 [8192, 512], P(('grp', 'sp'), 'tp'), parts along dimension 0, may hold values from -6 to 6
- value_rows: bfloat16 [8192, 512], P(('grp', 'sp'), 'tp'), parts along dimension 0, may hold values from -16 to 16
- key_bias: bfloat16 [8, 8192], P('tp', ('grp', 'sp')), parts along dimension 1, may hold values from -20 to 0
- residual: bfloat16 [8192, 2048], P(('grp', 'sp')), parts along dimension 0, may hold values from -6 to 6
- out_weight: bfloat16 [512, 2048], P('tp'), may hold values from -0.25 to 0.25
- norm_gain: bfloat16 [2048], replicated, may hold values from 0.099609375 to 1.8984375
- gate_weight: bfloat16 [2048, 3072], P('sp', 'tp'), may hold values from -0.125 to 0.125
- up_weight: bfloat16 [2048, 3072], P('sp', 'tp'), may hold values from -0.125 to 0.125
- down_weight: bfloat16 [3072, 2048], P('tp', 'sp'), may hold values from -0.109375 to 0.109375
Outputs:
- layer_out: bfloat16 [8192, 2048], P(('grp', 'sp')), parts along dimension 0
There are 2 independent parts, one for each index of `grp`. A program takes and returns all parts, laid end to end along the dimension named above; an argument that names none is the same for every part. Nothing has to cross between parts.
All inputs are finite; a program needn't handle non-finite values.
Results may differ from a plain program's by a relative error of at most 0.014.
Values may be sent and summed in bfloat16 or wider, within the bound.
No kernel may reach another device: no remote copies, remote signals or barrier semaphores. Data moves between devices by JAX's collectives and lax.ppermute only.
A program may use at most 64 MiB of HBM per device.

v0:
```python
import jax
import jax.numpy as jnp
from jax import lax
from jax.sharding import PartitionSpec as P

norm_eps = 1e-05


def side_by_side(arrays, axis, dim, along):
    both = jnp.concatenate(arrays, axis=along)
    out, at, done = (lax.all_gather(both, axis, axis=dim, tiled=True), 0, [])
    for a in arrays:
        done.append(lax.slice_in_dim(out, at, at + a.shape[along], axis=along))
        at += a.shape[along]
    return tuple(done)


def turned_gather(arrays, axis, dims):
    turned = [jnp.moveaxis(a, dim, 0) for a, dim in zip(arrays, dims)]
    widths = [t[0].size for t in turned]
    both = jnp.concatenate([t.reshape(-1, w) for t, w in zip(turned, widths)], axis=1)
    out = lax.all_gather(both, axis, axis=0, tiled=True)
    blocks = jnp.split(out, [sum(widths[:k]) for k in range(1, len(widths))], axis=1)
    return tuple(
        (
            jnp.moveaxis(b.reshape(-1, *t.shape[1:]), 0, dim)
            for b, t, dim in zip(blocks, turned, dims)
        )
    )


def cut_along(value, dim, length):
    shape = value.shape
    blocks = value.reshape(*shape[:dim], length, shape[dim] // length, *shape[dim + 1 :])
    return jnp.moveaxis(blocks, dim, 0)


def sum_at_owner(value, axis, dim):
    length = lax.axis_size(axis)
    blocks = lax.all_to_all(cut_along(value, dim, length), axis, 0, 0, tiled=True)
    return jnp.sum(blocks.astype(jnp.float32), axis=0)


def in_order(blocks, dim):
    blocks = jnp.moveaxis(blocks, 0, dim)
    shape = blocks.shape
    return blocks.reshape(*shape[:dim], shape[dim] * shape[dim + 1], *shape[dim + 2 :])


def sent_to_all(value, axis):
    copies = jnp.broadcast_to(value, (lax.axis_size(axis), *value.shape))
    return lax.all_to_all(copies, axis, split_axis=0, concat_axis=0, tiled=True)


def collect(value, axis, dim):
    return in_order(sent_to_all(value, axis), dim)


def stick_block(carry, query_heads, key_block, value_block, bias_block, query_pos, key_start):
    accum, kept_log = carry
    key_count = key_block.shape[0]
    head_count = query_heads.shape[1]
    key_heads = key_block.reshape(key_count, head_count, -1)
    value_heads = value_block.reshape(key_count, head_count, -1)
    scale = key_heads.shape[2] ** (-0.5)
    scores = (
        jnp.einsum("qhd,khd->hqk", query_heads, key_heads, preferred_element_type=jnp.float32)
        * scale
    )
    scores = scores + bias_block.astype(jnp.float32)[:, None, :]
    key_pos = key_start + lax.iota(jnp.int32, key_count)
    strict = ((key_pos[None, :] < query_pos[:, None]) & (key_pos[None, :] >= 0))[None]
    log_retained = jnp.where(strict, jax.nn.log_sigmoid(-scores), 0.0)
    between = lax.cumsum(log_retained, axis=2, reverse=True) - log_retained + kept_log[:, :, None]
    stick = jnp.where(strict, jnp.exp(jax.nn.log_sigmoid(scores) + between), 0.0).astype(
        jnp.bfloat16
    )
    accum = accum + jnp.einsum(
        "hqk,khd->qhd", stick, value_heads, preferred_element_type=jnp.float32
    )
    return (accum, kept_log + jnp.sum(log_retained, axis=2))


def normalize(middle_wide, norm_gain):
    mean_square = jnp.mean(middle_wide * middle_wide, axis=1, keepdims=True)
    return (middle_wide * lax.rsqrt(mean_square + norm_eps) * norm_gain.astype(jnp.float32)).astype(
        jnp.bfloat16
    )


def body(
    queries,
    key_rows,
    value_rows,
    key_bias,
    residual,
    out_weight,
    norm_gain,
    gate_weight,
    up_weight,
    down_weight,
):
    gate_full, up_full = side_by_side((gate_weight, up_weight), "sp", 0, 1)
    down_full = lax.all_gather(down_weight, "sp", axis=1, tiled=True)
    seg_rows = queries.shape[0]
    head_count = key_bias.shape[0]
    head_width = queries.shape[1] // head_count
    sp_count = lax.axis_size("sp")
    token_place = lax.axis_index("sp")
    query_heads = queries.reshape(seg_rows, head_count, head_width)
    query_pos = token_place * seg_rows + lax.iota(jnp.int32, seg_rows)
    start_carry = (
        jnp.zeros((seg_rows, head_count, head_width), jnp.float32),
        jnp.zeros((head_count, seg_rows), jnp.float32),
    )
    carry = stick_block(
        start_carry, query_heads, key_rows, value_rows, key_bias, query_pos, token_place * seg_rows
    )
    all_keys, all_values, all_bias = turned_gather(
        (key_rows, value_rows, key_bias), "sp", (0, 0, 1)
    )

    def visit(hop_index, carry_now):
        source = jnp.maximum(token_place - hop_index, 0)
        begin = source * seg_rows

        def attend(current):
            key_block = lax.dynamic_slice_in_dim(all_keys, begin, seg_rows, 0)
            value_block = lax.dynamic_slice_in_dim(all_values, begin, seg_rows, 0)
            bias_block = lax.dynamic_slice_in_dim(all_bias, begin, seg_rows, 1)
            return stick_block(
                current,
                query_heads,
                key_block,
                value_block,
                bias_block,
                query_pos,
                (token_place - hop_index) * seg_rows,
            )

        return lax.cond(token_place >= hop_index, attend, lambda current: current, carry_now)

    carry = lax.fori_loop(1, sp_count, visit, carry)
    attended = carry[0].reshape(seg_rows, head_count * head_width).astype(jnp.bfloat16)
    own_rows = seg_rows // lax.axis_size("tp")
    own_start = lax.axis_index("tp") * own_rows
    mixed = sum_at_owner(
        jnp.dot(attended, out_weight, preferred_element_type=jnp.float32).astype(jnp.bfloat16),
        "tp",
        0,
    )
    own_residual = lax.dynamic_slice_in_dim(residual, own_start, own_rows, 0)
    middle = (own_residual.astype(jnp.float32) + mixed).astype(jnp.bfloat16)
    middle_wide = middle.astype(jnp.float32)
    normed_all = collect(normalize(middle_wide, norm_gain), "tp", 0)
    gate_pre = jnp.dot(normed_all, gate_full, preferred_element_type=jnp.float32)
    up_pre = jnp.dot(normed_all, up_full, preferred_element_type=jnp.float32)
    hidden = (jax.nn.silu(gate_pre) * up_pre).astype(jnp.bfloat16)
    down_terms = jnp.dot(hidden, down_full, preferred_element_type=jnp.float32)
    down_sum = sum_at_owner(down_terms.astype(jnp.bfloat16), "tp", 0)
    own_out = (middle_wide + down_sum).astype(jnp.bfloat16)
    return collect(own_out, "tp", 0)


def solution(mesh):
    in_specs = (
        P(("grp", "sp"), "tp"),
        P(("grp", "sp"), "tp"),
        P(("grp", "sp"), "tp"),
        P("tp", ("grp", "sp")),
        P(("grp", "sp"), None),
        P("tp", None),
        P(),
        P("sp", "tp"),
        P("sp", "tp"),
        P("tp", "sp"),
    )
    out_specs = P(("grp", "sp"), None)
    return jax.shard_map(body, mesh=mesh, in_specs=in_specs, out_specs=out_specs, check_vma=False)
```

profile of v0, /device:TPU:40, one launch (start us, length us, event | category | flops | bytes accessed | tf_op | source)
XLA Modules:
  0.0 273.2 jit_solution(14697455399693322357)
XLA Ops:
  6.6 0.9 copy.20
  7.5 0.9 copy.21
  8.4 1.3 pad_maximum_fusion.1
  9.8 1.6 pad_maximum_fusion
  11.6 0.7 all-gather.8.cloned.1.call-update
  12.3 0.7 convert_element_type.61
  13.0 0.9 copy.19
  14.3 2.2 reduce_window_sum.17
  16.8 77.8 %all-gather.4.cloned.1.call-done = bf16[4096,258]{0,1:T(8,128)(2,1)} async-done(((bf16[128,258]{0,1:T(8,128)(2,1)}), bf16[4096,258]{0,1:T(8,128)(2,1)}) %all-gather.4.cloned.1.call-update) | async-done | bytes 2113552 | tf_op jit(solution)/shard_map/all_gather | solution.py:22
  94.7 0.8 slice_bitcast_fusion
  95.5 1.7 fusion.52
  97.2 1.6 while.16
  98.9 1.1 convolution_convert_fusion.1
  100.0 4.3 %all-to-all-start = ((bf16[4,32,2048]{2,1,0:T(8,128)(2,1)}), bf16[4,32,2048]{2,1,0:T(8,128)(2,1)S(1)}, u32[]{:S(2)}, u32[]{:S(2)}) async-start(bf16[4,32,2048]{2,1,0:T(8,128)(2,1)} %bitcast.11), calls=%async_computation | async-start | bytes 1048576 | tf_op jit(solution)/shard_map/all_to_all | solution.py:40
  104.3 8.8 %all-to-all-done = bf16[4,32,2048]{2,1,0:T(8,128)(2,1)S(1)} async-done(((bf16[4,32,2048]{2,1,0:T(8,128)(2,1)}), bf16[4,32,2048]{2,1,0:T(8,128)(2,1)S(1)}, u32[]{:S(2)}, u32[]{:S(2)}) %all-to-all-start) | async-done | bytes 524320 | tf_op jit(solution)/shard_map/all_to_all | solution.py:40
  113.2 1.1 fusion.36
  114.4 12.4 %all_to_all.20 = bf16[4,32,2048]{2,1,0:T(8,128)(2,1)S(1)} all-to-all(bf16[4,32,2048]{2,1,0:T(8,128)(2,1)S(1)} %broadcast_in_dim.46), channel_id=1, replica_groups=mesh['grp'=2,'sp'=32,'tp'=4] {'tp'}, dimensions={0} | all-to-all | bytes 1048576 | tf_op jit(solution)/shard_map/all_to_all | solution.py:52
  126.9 40.2 %all-gather.6.cloned.1.call-done = bf16[2048,1536]{1,0:T(8,128)(2,1)} async-done(((bf16[64,1536]{1,0:T(8,128)(2,1)}), bf16[2048,1536]{1,0:T(8,128)(2,1)}) %all-gather.6.cloned.1.call-update) | async-done | bytes 6291472 | tf_op jit(solution)/shard_map/all_gather | solution.py:11
  167.1 2.5 fusion.20
  169.6 66.3 %all-gather.8.cloned.1.call-done = bf16[768,2048]{0,1:T(8,128)(2,1)} async-done(((bf16[768,64]{0,1:T(8,128)(2,1)}), bf16[768,2048]{0,1:T(8,128)(2,1)}) %all-gather.8.cloned.1.call-update) | async-done | bytes 3145744 | tf_op jit(solution)/shard_map/all_gather | solution.py:104
  235.8 4.5 %convolution_convert_fusion = bf16[128,2048]{1,0:T(8,128)(2,1)S(1)} fusion(bf16[768,2048]{0,1:T(8,128)(2,1)} %all-gather.8.cloned.1.call-done, bf16[128,2048]{1,0:T(8,128)(2,1)S(1)} %bitcast.36, bf16[2048,1536]{1,0:T(8,128)(2,1)} %all-gather.6.cloned.1.call-done, f32[128,768]{1,0:T(8,128)S(1)} %fusion.20), kind=kOutput, calls=%fused_computation.30 | convolution fusion | flops 806158336 | bytes 7733248 | tf_op jit(solution)/shard_map/dot_general | solution.py:159
  240.3 13.9 %all_to_all.21 = bf16[4,32,2048]{2,1,0:T(8,128)(2,1)S(1)} all-to-all(bf16[4,32,2048]{2,1,0:T(8,128)(2,1)S(1)} %bitcast.37), channel_id=1, replica_groups=mesh['grp'=2,'sp'=32,'tp'=4] {'tp'}, dimensions={0} | all-to-all | bytes 1048576 | tf_op jit(solution)/shard_map/all_to_all | solution.py:40
  254.4 11.4 %all_to_all.22 = bf16[4,32,2048]{2,1,0:T(8,128)(2,1)S(1)} all-to-all(bf16[4,32,2048]{2,1,0:T(8,128)(2,1)S(1)} %broadcast_in_dim.47), channel_id=1, replica_groups=mesh['grp'=2,'sp'=32,'tp'=4] {'tp'}, dimensions={0} | all-to-all | bytes 1048576 | tf_op jit(solution)/shard_map/all_to_all | solution.py:52
  265.9 0.8 copy.41
  (86 shorter events, 1.9 us)
Async XLA Ops:
  6.5 92.3 %copy-start = (bf16[128,2048]{1,0:T(8,128)(2,1)S(1)}, bf16[128,2048]{1,0:T(8,128)(2,1)}, u32[]{:S(2)}) copy-start(bf16[128,2048]{1,0:T(8,128)(2,1)} %param.19) | copy-start | bytes 1572868
  6.6 88.1 %all-gather.4.cloned.1.call-start = ((), (), s32[]{:S(2)}) async-start(), calls=%async_computation.4 | async-start | bytes 2230272 | tf_op jit(solution)/shard_map/all_gather | solution.py:22
  9.7 157.4 %all-gather.6.cloned.1.call-start = ((), (), s32[]{:S(2)}) async-start(), calls=%async_computation.5 | async-start | bytes 6488064 | tf_op jit(solution)/shard_map/all_gather | solution.py:11
  11.5 224.3 %all-gather.8.cloned.1.call-start = ((), (), s32[]{:S(2)}) async-start(), calls=%async_computation.6 | async-start | bytes 3244032 | tf_op jit(solution)/shard_map/all_gather | solution.py:104
  97.2 7.1 %copy-start.1 = (bf16[2048]{0:T(1024)(128)(2,1)S(1)}, bf16[2048]{0:T(1024)(128)(2,1)}, u32[]{:S(2)}) copy-start(bf16[2048]{0:T(1024)(128)(2,1)} %param.20) | copy-start | bytes 12292
  100.0 13.1 %all-to-all-start = ((bf16[4,32,2048]{2,1,0:T(8,128)(2,1)}), bf16[4,32,2048]{2,1,0:T(8,128)(2,1)S(1)}, u32[]{:S(2)}, u32[]{:S(2)}) async-start(bf16[4,32,2048]{2,1,0:T(8,128)(2,1)} %bitcast.11), calls=%async_computation | async-start | bytes 1048576 | tf_op jit(solution)/shard_map/all_to_all | solution.py:40
Sparse Core Ops, SparseCore 0:
  9.8 84.7 all-gather.3
  96.5 70.5 all-gather.5
  168.9 66.8 all-gather.7
where the time goes:
time: 274 us; the launch traced here: 273 us
  waiting for transfers between devices  194 us (71%)
  blocking collectives  37.8 us (14%)
  between operations  13.3 us (5%)
  matrix products  8.63 us (3%)
  other arithmetic  7.43 us (3%)
  local copies, waits for them, and re-layouts  6.15 us (2%)
  starting transfers between devices  4.39 us (2%)
    all_gather x1, waiting for transfers between devices, turned_gather(): out = lax.all_gather(both, axis, axis=0, tiled=True)  77.8 us
    all_gather x1, waiting for transfers between devices, body(): down_full = lax.all_gather(down_weight, 'sp', axis=1, tiled=True)  66.3 us
    all_gather x1, waiting for transfers between devices, side_by_side(): out, at, done = (lax.all_gather(both, axis, axis=dim, tiled=True), 0, [])  40.2 us
    all_to_all x2, blocking collectives, sent_to_all(): return lax.all_to_all(copies, axis, split_axis=0, concat_axis=0, tiled=True)  23.9 us
    all_to_all x1, blocking collectives, sum_at_owner(): lax.all_to_all(cut_along(value, dim, length), axis, 0, 0, tiled=True)  13.9 us
    all_to_all x1, waiting for transfers between devices, sum_at_owner(): lax.all_to_all(cut_along(value, dim, length), axis, 0, 0, tiled=True)  8.84 us
  transfers between devices with their start and end apart: 4, of which 4 were waited for; matrix products, arithmetic and copies ran while one was open for 5% of the time, Pallas kernels for 0%

commit v1 on v0

--- a/solution.py
+++ b/solution.py
@@ -101,7 +101,9 @@
     down_weight,
 ):
     gate_full, up_full = side_by_side((gate_weight, up_weight), "sp", 0, 1)
-    down_full = lax.all_gather(down_weight, "sp", axis=1, tiled=True)
+    down_full = jnp.concatenate(
+        lax.all_to_all(jnp.stack([down_weight] * lax.axis_size("sp")), "sp", 0, 0), axis=1
+    )
     seg_rows = queries.shape[0]
     head_count = key_bias.shape[0]
     head_width = queries.shape[1] // head_count

time: 274 us -> 438 us (1.60)
  starting transfers between devices: 4.39 us -> 104 us
  waiting for transfers between devices: 194 us -> 264 us
  blocking collectives: 37.8 us -> 29.1 us
    all_gather x1, waiting for transfers between devices: 40.2 us -> 161 us  [side_by_side(): out, at, done = (lax.all_gather(both, axis, axis=dim, tiled=True), 0, [])]
    all_to_all x0 -> x2, starting transfers between devices: none -> 100 us  [the longest x1 96.4 us: body(): lax.all_to_all(jnp.stack([down_weight] * lax.axis_size('sp')), 'sp', 0, 0)]
    all_gather x1 -> x0, waiting for transfers between devices: 66.3 us -> none  [body(): down_full = lax.all_gather(down_weight, 'sp', axis=1, tiled=True)]
    all_to_all x0 -> x2, waiting for transfers between devices: none -> 13.5 us  [the longest x1 9.06 us: sent_to_all(): return lax.all_to_all(copies, axis, split_axis=0, concat_axis=0, tiled=True)]
    all_to_all x2 -> x1, blocking collectives: 23.9 us -> 11 us  [sent_to_all(): return lax.all_to_all(copies, axis, split_axis=0, concat_axis=0, tiled=True)]
  transfers between devices with their start and end apart: 4 -> 5, of which waited for: 4 -> 5; matrix products, arithmetic and copies ran while one was open for 5% -> 2% of each run, Pallas kernels for 0% -> 0%
where the time goes in v1:
time: 438 us; the launch traced here: 437 us
  waiting for transfers between devices  264 us (60%)
  starting transfers between devices  104 us (24%)
  blocking collectives  29.1 us (7%)
  between operations  13.6 us (3%)
  local copies, waits for them, and re-layouts  8.96 us (2%)
  matrix products  8.67 us (2%)
  other arithmetic  6.47 us (1%)
    all_gather x1, waiting for transfers between devices, side_by_side(): out, at, done = (lax.all_gather(both, axis, axis=dim, tiled=True), 0, [])  161 us
    all_to_all x1, starting transfers between devices, body(): lax.all_to_all(jnp.stack([down_weight] * lax.axis_size('sp')), 'sp', 0, 0)  96.4 us
    all_gather x1, waiting for transfers between devices, turned_gather(): out = lax.all_gather(both, axis, axis=0, tiled=True)  80.4 us
    all_to_all x1, blocking collectives, sum_at_owner(): lax.all_to_all(cut_along(value, dim, length), axis, 0, 0, tiled=True)  18.1 us
    all_to_all x1, blocking collectives, sent_to_all(): return lax.all_to_all(copies, axis, split_axis=0, concat_axis=0, tiled=True)  11 us
    all_to_all x1, waiting for transfers between devices, sent_to_all(): return lax.all_to_all(copies, axis, split_axis=0, concat_axis=0, tiled=True)  9.06 us
    all_to_all x1, waiting for transfers between devices, sum_at_owner(): lax.all_to_all(cut_along(value, dim, length), axis, 0, 0, tiled=True)  8.85 us
  transfers between devices with their start and end apart: 5, of which 5 were waited for; matrix products, arithmetic and copies ran while one was open for 2% of the time, Pallas kernels for 0%

profile of v1, /device:TPU:40, one launch (start us, length us, event | category | flops | bytes accessed | tf_op | source)
XLA Modules:
  0.0 437.0 jit_solution(13688144661076011974)
XLA Ops:
  6.6 0.9 copy.22
  7.5 0.9 copy.21
  8.4 1.3 pad_maximum_fusion.1
  10.4 0.9 copy.20
  11.7 2.2 reduce_window_sum.17
  14.3 80.4 %all-gather.3.cloned.1.call-done = bf16[4096,258]{0,1:T(8,128)(2,1)} async-done(((bf16[128,258]{0,1:T(8,128)(2,1)}), bf16[4096,258]{0,1:T(8,128)(2,1)}) %all-gather.3.cloned.1.call-update) | async-done | bytes 2113552 | tf_op jit(solution)/shard_map/all_gather | solution.py:22
  94.7 1.7 fusion.52
  96.3 0.9 slice_bitcast_fusion
  97.2 1.6 while.16
  98.9 1.1 convolution_convert_fusion.1
  100.0 4.3 all-to-all-start
  104.3 8.8 %all-to-all-done = bf16[4,32,2048]{2,1,0:T(8,128)(2,1)S(1)} async-done(((bf16[4,32,2048]{2,1,0:T(8,128)(2,1)}), bf16[4,32,2048]{2,1,0:T(8,128)(2,1)S(1)}, u32[]{:S(2)}, u32[]{:S(2)}) %all-to-all-start) | async-done | bytes 524320 | tf_op jit(solution)/shard_map/all_to_all | solution.py:40
  113.2 1.1 fusion.36
  114.4 0.8 broadcast_in_dim.46
  115.3 3.6 all-to-all-start.1
  119.7 9.1 %all-to-all-done.1 = bf16[4,32,2048]{2,1,0:T(8,128)(2,1)S(1)} async-done(((bf16[4,32,2048]{2,1,0:T(8,128)(2,1)}), bf16[4,32,2048]{2,1,0:T(8,128)(2,1)S(1)}, u32[]{:S(2)}, u32[]{:S(2)}) %all-to-all-start.1) | async-done | bytes 524320 | tf_op jit(solution)/shard_map/all_to_all | solution.py:52
  128.7 2.0 stack.2
  130.7 96.4 %all-to-all-start.2 = ((bf16[32,768,64]{1,2,0:T(8,128)(2,1)}), bf16[32,768,64]{1,2,0:T(8,128)(2,1)}, u32[]{:S(2)}, u32[]{:S(2)}) async-start(bf16[32,768,64]{1,2,0:T(8,128)(2,1)} %stack.2), calls=%async_computation.2 | async-start | bytes 6291456 | tf_op jit(solution)/shard_map/all_to_all | solution.py:105
  227.1 161.5 %all-gather.5.cloned.1.call-done = bf16[2048,1536]{1,0:T(8,128)(2,1)} async-done(((bf16[64,1536]{1,0:T(8,128)(2,1)}), bf16[2048,1536]{1,0:T(8,128)(2,1)}) %all-gather.5.cloned.1.call-update) | async-done | bytes 6291472 | tf_op jit(solution)/shard_map/all_gather | solution.py:11
  388.6 2.5 fusion.20
  391.1 4.4 %all-to-all-done.2 = bf16[32,768,64]{1,2,0:T(8,128)(2,1)} async-done(((bf16[32,768,64]{1,2,0:T(8,128)(2,1)}), bf16[32,768,64]{1,2,0:T(8,128)(2,1)}, u32[]{:S(2)}, u32[]{:S(2)}) %all-to-all-start.2) | async-done | bytes 3145760 | tf_op jit(solution)/shard_map/all_to_all | solution.py:105
  395.5 4.5 %convolution_convert_fusion = bf16[128,2048]{1,0:T(8,128)(2,1)S(1)} fusion(bf16[768,2048]{0,1:T(8,128)(2,1)} %bitcast.14, bf16[128,2048]{1,0:T(8,128)(2,1)S(1)} %bitcast.39, bf16[2048,1536]{1,0:T(8,128)(2,1)} %all-gather.5.cloned.1.call-done, f32[128,768]{1,0:T(8,128)S(1)} %fusion.20), kind=kOutput, calls=%fused_computation.30 | convolution fusion | flops 806158336 | bytes 7733248 | tf_op jit(solution)/shard_map/dot_general | solution.py:161
  400.1 18.1 %all_to_all.25 = bf16[4,32,2048]{2,1,0:T(8,128)(2,1)S(1)} all-to-all(bf16[4,32,2048]{2,1,0:T(8,128)(2,1)S(1)} %bitcast.40), channel_id=1, replica_groups=mesh['grp'=2,'sp'=32,'tp'=4] {'tp'}, dimensions={0} | all-to-all | bytes 1048576 | tf_op jit(solution)/shard_map/all_to_all | solution.py:40
  418.3 11.0 %all_to_all.26 = bf16[4,32,2048]{2,1,0:T(8,128)(2,1)S(1)} all-to-all(bf16[4,32,2048]{2,1,0:T(8,128)(2,1)S(1)} %broadcast_in_dim.47), channel_id=1, replica_groups=mesh['grp'=2,'sp'=32,'tp'=4] {'tp'}, dimensions={0} | all-to-all | bytes 1048576 | tf_op jit(solution)/shard_map/all_to_all | solution.py:52
  (93 shorter events, 4.0 us)
Async XLA Ops:
  6.5 92.4 %copy-start = (bf16[128,2048]{1,0:T(8,128)(2,1)S(1)}, bf16[128,2048]{1,0:T(8,128)(2,1)}, u32[]{:S(2)}) copy-start(bf16[128,2048]{1,0:T(8,128)(2,1)} %param.19) | copy-start | bytes 1572868
  6.6 88.1 %all-gather.3.cloned.1.call-start = ((), (), s32[]{:S(2)}) async-start(), calls=%async_computation.5 | async-start | bytes 2230272 | tf_op jit(solution)/shard_map/all_gather | solution.py:22
  97.2 7.1 %copy-start.4 = (bf16[2048]{0:T(1024)(128)(2,1)S(1)}, bf16[2048]{0:T(1024)(128)(2,1)}, u32[]{:S(2)}) copy-start(bf16[2048]{0:T(1024)(128)(2,1)} %param.20) | copy-start | bytes 12292
  98.9 20.1 %copy-start.2 = (bf16[64,768]{1,0:T(8,128)(2,1)S(1)}, bf16[64,768]{1,0:T(8,128)(2,1)}, u32[]{:S(2)}) copy-start(bf16[64,768]{1,0:T(8,128)(2,1)} %param.22) | copy-start | bytes 294916
  98.9 20.0 %copy-start.3 = (bf16[64,768]{1,0:T(8,128)(2,1)S(1)}, bf16[64,768]{1,0:T(8,128)(2,1)}, u32[]{:S(2)}) copy-start(bf16[64,768]{1,0:T(8,128)(2,1)} %param.21) | copy-start | bytes 294916
  98.9 29.9 %copy-start.1 = (bf16[768,64]{0,1:T(8,128)(2,1)S(1)}, bf16[768,64]{0,1:T(8,128)(2,1)}, u32[]{:S(2)}) copy-start(bf16[768,64]{0,1:T(8,128)(2,1)} %param.23) | copy-start | bytes 294916
  100.0 13.1 %all-to-all-start = ((bf16[4,32,2048]{2,1,0:T(8,128)(2,1)}), bf16[4,32,2048]{2,1,0:T(8,128)(2,1)S(1)}, u32[]{:S(2)}, u32[]{:S(2)}) async-start(bf16[4,32,2048]{2,1,0:T(8,128)(2,1)} %bitcast.11), calls=%async_computation | async-start | bytes 1048576 | tf_op jit(solution)/shard_map/all_to_all | solution.py:40
  115.3 13.5 %all-to-all-start.1 = ((bf16[4,32,2048]{2,1,0:T(8,128)(2,1)}), bf16[4,32,2048]{2,1,0:T(8,128)(2,1)S(1)}, u32[]{:S(2)}, u32[]{:S(2)}) async-start(bf16[4,32,2048]{2,1,0:T(8,128)(2,1)} %broadcast_in_dim.46), calls=%async_computation.1 | async-start | bytes 1048576 | tf_op jit(solution)/shard_map/all_to_all | solution.py:52
  118.8 269.8 %all-gather.5.cloned.1.call-start = ((), (), s32[]{:S(2)}) async-start(), calls=%async_computation.6 | async-start | bytes 6488064 | tf_op jit(solution)/shard_map/all_gather | solution.py:11
  130.7 264.8 %all-to-all-start.2 = ((bf16[32,768,64]{1,2,0:T(8,128)(2,1)}), bf16[32,768,64]{1,2,0:T(8,128)(2,1)}, u32[]{:S(2)}, u32[]{:S(2)}) async-start(bf16[32,768,64]{1,2,0:T(8,128)(2,1)} %stack.2), calls=%async_computation.2 | async-start | bytes 6291456 | tf_op jit(solution)/shard_map/all_to_all | solution.py:105
Sparse Core Ops, SparseCore 0:
  9.8 84.7 all-gather.2
  121.5 267.0 all-gather.4
